TPU v7x, 128 devices: a 2x2x16 block of a 8x8x16 slice. The times are simulated.
128 devices in a mesh: grp: 4 (over y, x), ep: 32 (over z, core).
Axes of the slice: x: 2, y: 2, z: 16, core: 2. Of those that a mesh axis runs over, the one named last changes fastest.
The devices are a block of a 8x8x16 slice.
Arguments:
- tokens: bfloat16 [4096, 2048], P(('grp', 'ep')), parts along dimension 0, may hold values from -6 to 6
- routes: int32 [4096, 4], P(('grp', 'ep')), parts along dimension 0, may hold values from 0 to 31, all different within a row; in each aligned block of 32 rows (0 to 31, 32 to 63, ...) at most 8 rows name the same one
- route_logits: float32 [4096, 4], P(('grp', 'ep')), parts along dimension 0, may hold values from -4 to 4
- state_real: float32 [4096, 64, 64], P('grp', 'ep'), parts along dimension 0, may hold values from -4 to 4
- state_imag: float32 [4096, 64, 64], P('grp', 'ep'), parts along dimension 0, may hold values from -4 to 4
- gain_in: float32 [2048], replicated, may hold values from 0.1 to 1.9
- proj_in: bfloat16 [2048, 1024], P(None, 'ep'), may hold values from -0.125 to 0.125
- decay_rate: float32 [64, 64], P('ep'), may hold values from 0.05 to 2
- frequency: float32 [64, 64], P('ep'), may hold values from -4 to 4
- log_step: float32 [64], P('ep'), may hold values from -3 to 0
- input_real: float32 [64, 64, 16], P('ep'), may hold values from -1 to 1
- input_imag: float32 [64, 64, 16], P('ep'), may hold values from -1 to 1
- output_real: float32 [64, 16, 64], P('ep'), may hold values from -0.5 to 0.5
- output_imag: float32 [64, 16, 64], P('ep'), may hold values from -0.5 to 0.5
- skip_gain: float32 [64, 16], P('ep'), may hold values from -4 to 4
- proj_out: bfloat16 [1024, 2048], P('ep'), may hold values from -0.1875 to 0.1875
- gain_mid: float32 [2048], replicated, may hold values from 0.1 to 1.9
- expert_gate: bfloat16 [32, 2048, 1024], P('ep'), may hold values from -0.33007812 to 0.33007812
- expert_up: bfloat16 [32, 2048, 1024], P('ep'), may hold values from -0.33007812 to 0.33007812
- expert_down: bfloat16 [32, 1024, 2048], P('ep'), may hold values from -0.056152344 to 0.056152344
- dense_gate: bfloat16 [2048, 2048], P(None, 'ep'), may hold values from -0.125 to 0.125
- dense_up: bfloat16 [2048, 2048], P(None, 'ep'), may hold values from -0.125 to 0.125
- dense_down: bfloat16 [2048, 2048], P('ep'), may hold values from -0.125 to 0.125
- dense_mix: float32 [2048], P('ep'), may hold values from -0.39774758 to 0.39774758
Outputs:
- layer_out: bfloat16 [4096, 2048], P(('grp', 'ep')), parts along dimension 0
- state_real_new: float32 [4096, 64, 64], P('grp', 'ep'), parts along dimension 0
- state_imag_new: float32 [4096, 64, 64], P('grp', 'ep'), parts along dimension 0
There are 4 independent parts, one for each index of `grp`. A program takes and returns all parts, laid end to end along the dimension named above; an argument that names none is the same for every part. Nothing has to cross between parts.
Inputs may be any that keep to these rules, and one draw needn't show every extreme that they name: `routes`: each row names 4 different experts; among the rows of one device no expert is named more than 8 times, and in every draw some device names some expert exactly 8 times.
All inputs are finite; a program needn't handle non-finite values.
Results may differ from a plain program's by a relative error of at most 0.015.
Values may be sent and summed in bfloat16 or wider, within the bound.
A program may use at most 128 MiB of HBM per device.

v0:
```python
import jax
import jax.numpy as jnp
from jax import lax
from jax.sharding import Mesh
from jax.sharding import PartitionSpec as P

EP = ("ep_0", "ep_1")
GRP_EP = ("grp", "ep_0", "ep_1")


EPS = 1e-06
LIMIT = 7.0
ALPHA = 1.702


def copy_for_each(shard, axis):
    length = lax.axis_size(axis)
    return lax.all_to_all(
        jnp.broadcast_to(shard[None], (length, *shard.shape)), axis, 0, 0, tiled=True
    )


def of_everyone(shard, axis):
    return copy_for_each(shard, axis).sum(axis=0)


def reduced_to_own(blocks, axes, turns):
    lengths = [lax.axis_size(a) for a in axes]
    blocks = blocks.reshape(*lengths, *blocks.shape[1:])
    blocks = blocks.transpose(*turns, *range(len(axes), blocks.ndim))
    blocks = blocks.reshape(-1, *blocks.shape[len(axes) :])
    for k in turns:
        blocks = lax.psum_scatter(blocks, axes[k], scatter_dimension=0, tiled=True)
    return blocks[0]


def split_up(shard, dim, length):
    before, after = (shard.shape[:dim], shard.shape[dim + 1 :])
    return jnp.moveaxis(shard.reshape(*before, length, -1, *after), dim, 0)


def scatter_axes(shard, axes, turns, dim):
    length = lax.axis_size(axes)
    return reduced_to_own(split_up(shard, dim, length), axes, turns)


def rms_scale(values, gain_vec):
    return values * lax.rsqrt(jnp.mean(values * values, axis=-1, keepdims=True) + EPS) * gain_vec


def state_step(
    unit_rows,
    state_real,
    state_imag,
    decay_rate,
    frequency,
    log_step,
    input_real,
    input_imag,
    output_real,
    output_imag,
    skip_gain,
):
    seq_count = unit_rows.shape[0]
    groups, group_size = skip_gain.shape
    inputs = unit_rows.astype(jnp.float32).reshape(seq_count, groups, group_size)
    step_size = jnp.exp(log_step)[:, None]
    decay_part = -decay_rate
    magnitude = jnp.exp(decay_part * step_size)
    carry_real = magnitude * jnp.cos(frequency * step_size)
    carry_imag = magnitude * jnp.sin(frequency * step_size)
    denom = decay_part * decay_part + frequency * frequency
    feed_real = ((carry_real - 1.0) * decay_part + carry_imag * frequency) / denom
    feed_imag = (carry_imag * decay_part - (carry_real - 1.0) * frequency) / denom
    drive_real = jnp.einsum("sgp,gnp->sgn", inputs, input_real)
    drive_imag = jnp.einsum("sgp,gnp->sgn", inputs, input_imag)
    new_real = (
        carry_real * state_real
        - carry_imag * state_imag
        + feed_real * drive_real
        - feed_imag * drive_imag
    )
    new_imag = (
        carry_real * state_imag
        + carry_imag * state_real
        + feed_real * drive_imag
        + feed_imag * drive_real
    )
    readout = (
        jnp.einsum("gpn,sgn->sgp", output_real, new_real)
        - jnp.einsum("gpn,sgn->sgp", output_imag, new_imag)
        + skip_gain * inputs
    )
    branch = jax.nn.gelu(readout).reshape(seq_count, groups * group_size).astype(jnp.bfloat16)
    return (branch, new_real, new_imag)


def expert_apply(row_block, gate_weight, up_weight, down_weight):
    gated = jnp.minimum(jnp.dot(row_block, gate_weight, preferred_element_type=jnp.float32), LIMIT)
    upper = jnp.clip(
        jnp.dot(row_block, up_weight, preferred_element_type=jnp.float32), -LIMIT, LIMIT
    )
    activated = ((upper + 1.0) * gated * jax.nn.sigmoid(ALPHA * gated)).astype(jnp.bfloat16)
    return jnp.dot(activated, down_weight, preferred_element_type=jnp.float32).astype(jnp.bfloat16)


def dense_hidden(row_block, dense_gate, dense_up):
    return (
        jax.nn.silu(jnp.dot(row_block, dense_gate, preferred_element_type=jnp.float32))
        * jnp.dot(row_block, dense_up, preferred_element_type=jnp.float32)
    ).astype(jnp.bfloat16)


def on_device(
    tokens,
    routes,
    route_logits,
    state_real,
    state_imag,
    gain_in,
    proj_in,
    decay_rate,
    frequency,
    log_step,
    input_real,
    input_imag,
    output_real,
    output_imag,
    skip_gain,
    proj_out,
    gain_mid,
    expert_gate,
    expert_up,
    expert_down,
    dense_gate,
    dense_up,
    dense_down,
    dense_mix,
):
    devices = lax.axis_size(EP)
    own_rows = tokens.shape[0]
    top_count = routes.shape[1]
    capacity = max(2, 2 * own_rows * top_count // devices)
    inputs = tokens.astype(jnp.float32)
    normed = rms_scale(inputs, gain_in).astype(jnp.bfloat16)
    unit_rows = jnp.dot(
        lax.all_gather(normed, EP, axis=0, tiled=True), proj_in, preferred_element_type=jnp.float32
    ).astype(jnp.bfloat16)
    branch, new_real, new_imag = state_step(
        unit_rows,
        state_real,
        state_imag,
        decay_rate,
        frequency,
        log_step,
        input_real,
        input_imag,
        output_real,
        output_imag,
        skip_gain,
    )
    whole_out = lax.all_gather(proj_out, EP, axis=0, tiled=True)
    own_branch = lax.all_to_all(branch, EP, split_axis=0, concat_axis=1, tiled=True)
    mixer_out = jnp.dot(own_branch, whole_out, preferred_element_type=jnp.float32)
    residual = inputs + mixer_out
    mixed = rms_scale(residual, gain_mid).astype(jnp.bfloat16)
    weights = jnp.exp(route_logits)
    weights = weights / jnp.sum(weights, axis=1, keepdims=True)
    whole_rows = lax.all_gather(mixed, EP, axis=0, tiled=True)
    hidden = dense_hidden(whole_rows, dense_gate, dense_up)
    logit_term = jnp.dot(hidden.astype(jnp.float32), dense_mix)
    expert_ids = jnp.arange(devices, dtype=jnp.int32)
    shares = jnp.sum(
        jnp.where(routes[:, :, None] == expert_ids[None, None, :], weights[:, :, None], 0.0), axis=1
    )
    my_shares = lax.all_to_all(shares, EP, split_axis=1, concat_axis=0, tiled=True)[:, 0]
    gate_logit = of_everyone(logit_term, EP)
    marked = (my_shares > 0.0).astype(jnp.int32)
    rank_rows = jnp.cumsum(marked) - 1
    slot_ids = jnp.arange(devices * capacity, dtype=jnp.int32)
    selector = ((rank_rows[None, :] == slot_ids[:, None]) & (marked[None, :] == 1)).astype(
        jnp.bfloat16
    )
    picked = jnp.dot(selector, whole_rows, preferred_element_type=jnp.float32).astype(jnp.bfloat16)
    result = expert_apply(picked, expert_gate[0], expert_up[0], expert_down[0])
    expert_term = my_shares[:, None] * jnp.dot(
        selector.T, result, preferred_element_type=jnp.float32
    )
    gate_weight = jax.nn.sigmoid(gate_logit)
    dense_part = jnp.dot(hidden, dense_down, preferred_element_type=jnp.float32)
    combined = scatter_axes(
        (gate_weight[:, None] * dense_part + expert_term).astype(jnp.bfloat16), EP, (1, 0), 0
    ).astype(jnp.float32)
    layer_out = (residual + combined).astype(jnp.bfloat16)
    return (layer_out, new_real, new_imag)


def solution(mesh):
    split = Mesh(mesh.devices.reshape(mesh.shape["grp"], 16, 2), ("grp", "ep_0", "ep_1"))
    return jax.shard_map(
        on_device,
        mesh=split,
        in_specs=(
            P(GRP_EP, None),
            P(GRP_EP, None),
            P(GRP_EP, None),
            P("grp", EP, None),
            P("grp", EP, None),
            P(),
            P(None, EP),
            P(EP, None),
            P(EP, None),
            P(EP),
            P(EP, None, None),
            P(EP, None, None),
            P(EP, None, None),
            P(EP, None, None),
            P(EP, None),
            P(EP, None),
            P(),
            P(EP, None, None),
            P(EP, None, None),
            P(EP, None, None),
            P(None, EP),
            P(None, EP),
            P(EP, None),
            P(EP),
        ),
        out_specs=(P(GRP_EP, None), P("grp", EP, None), P("grp", EP, None)),
        check_vma=False,
    )
```

profile of v0, /device:TPU:86, one launch (start us, length us, event | category | flops | bytes accessed | tf_op | source)
XLA Modules:
  0.0 369.3 jit_solution(18087104272636381109)
XLA Ops:
  7.2 0.0 copy-start
  7.2 0.1 all-gather.4.cloned.1.call-start
  7.3 1.1 fusion.39
  8.4 1.7 fusion.41
  10.1 0.1 all-gather.4.cloned.1.call-update
  10.2 0.1 all-gather.6.cloned.1.call-start
  10.2 0.7 all-gather.6.cloned.1.call-update
  11.0 0.1 all-gather.8.cloned.1.call-start
  11.1 0.7 exp.23
  11.7 0.8 cosine_multiply_fusion
  12.5 0.0 copy-start.10
  12.6 0.0 copy-start.15
  12.6 73.8 %all-gather.4.cloned.1.call-done = bf16[1024,2048]{1,0:T(8,128)(2,1)} async-done(((bf16[32,2048]{1,0:T(8,128)(2,1)}), bf16[1024,2048]{1,0:T(8,128)(2,1)}) %all-gather.4.cloned.1.call-update) | async-done | bytes 4194320 | tf_op jit(solution)/shard_map/all_gather | solution.py:147
  86.4 3.5 convolution_convert_fusion.1
  89.9 0.0 copy-start.4
  89.9 0.3 fusion.58
  90.2 0.4 bitcast_add_fusion
  90.6 0.0 copy-start.2
  90.6 0.0 copy-start.3
  90.7 0.2 fusion.59
  90.9 0.2 fusion.50
  91.1 0.2 convert_element_type.63
  91.3 0.3 copy.43
  91.6 0.2 reshape.129
  91.8 23.2 %all_to_all.38 = bf16[32,2,512]{2,1,0:T(2,128)(2,1)S(1)} all-to-all(bf16[32,2,512]{2,1,0:T(2,128)(2,1)S(1)} %reshape.129), channel_id=1, replica_groups=mesh['grp'=4,'ep_0'=16,'ep_1'=2] {'ep_0','ep_1'}, dimensions={0} | all-to-all | bytes 131072 | tf_op jit(solution)/shard_map/all_to_all | solution.py:163
  115.1 0.2 reshape.130
  115.3 0.1 copy.44
  115.4 0.3 all_to_all.30
  115.6 41.1 %all-gather.6.cloned.1.call-done = bf16[1024,2048]{1,0:T(8,128)(2,1)} async-done(((bf16[32,2048]{1,0:T(8,128)(2,1)}), bf16[1024,2048]{1,0:T(8,128)(2,1)}) %all-gather.6.cloned.1.call-update) | async-done | bytes 4194320 | tf_op jit(solution)/shard_map/all_gather | solution.py:162
  156.7 3.1 multiply_reduce_fusion
  159.9 0.7 multiply_convert_fusion
  160.6 0.1 all-gather.8.cloned.1.call-update
  160.8 0.1 select_reduce_fusion
  160.9 0.1 copy.46
  160.9 19.4 %all_to_all.39 = f32[32,32,1]{0,2,1:T(1,128)S(1)} all-to-all(f32[32,32,1]{0,2,1:T(1,128)S(1)} %copy.46), channel_id=1, replica_groups=mesh['grp'=4,'ep_0'=16,'ep_1'=2] {'ep_0','ep_1'}, dimensions={1} | all-to-all | bytes 8192 | tf_op jit(solution)/shard_map/all_to_all | solution.py:176
  180.4 0.1 fusion.51
  180.4 0.1 reshape.109
  180.5 0.1 mul.264
  180.6 0.3 reduce-window.9
  180.9 0.1 slice.7
  181.0 0.1 slice_reduce_fusion
  181.1 0.1 add_bitcast_fusion
  181.2 45.6 %all-gather.8.cloned.1.call-done = bf16[1024,2048]{1,0:T(8,128)(2,1)} async-done(((bf16[32,2048]{1,0:T(8,128)(2,1)}), bf16[1024,2048]{1,0:T(8,128)(2,1)}) %all-gather.8.cloned.1.call-update) | async-done | bytes 4194320 | tf_op jit(solution)/shard_map/all_gather | solution.py:169
  226.8 3.7 %fusion.60 = f32[1024,64]{0,1:T(8,128)S(1)} fusion(bf16[1024,2048]{1,0:T(8,128)(2,1)} %all-gather.8.cloned.1.call-done, bf16[2048,64]{0,1:T(8,128)(2,1)S(1)} %copy-done.7), kind=kOutput, calls=%fused_computation.75 | convolution fusion | flops 268435456 | bytes 4718592 | tf_op jit(solution)/shard_map/dot_general | solution.py:109
  230.5 1.4 fusion.27
  231.9 0.1 fusion.55
  232.1 0.7 broadcast_in_dim.10
  232.8 9.0 %all-to-all-start.1 = ((f32[32,1,1024]{2,1,0:T(1,128)}), f32[32,1,1024]{2,1,0:T(1,128)S(1)}, u32[]{:S(2)}, u32[]{:S(2)}) async-start(f32[32,1,1024]{2,1,0:T(1,128)} %broadcast_in_dim.10), calls=%async_computation.1 | async-start | bytes 262144 | tf_op jit(solution)/shard_map/all_to_all | solution.py:18
  241.9 0.2 reduce-scatter.3.cloned.1.call-start
  242.1 3.6 convolution_convert_fusion
  245.7 1.3 fusion.9
  247.0 0.9 copy-done.18
  247.9 1.4 fusion.24
  249.4 4.5 %fusion.61 = f32[1024,2048]{1,0:T(8,128)} fusion(bf16[1024,64]{0,1:T(8,128)(2,1)S(1)} %fusion.27, bf16[64,2048]{1,0:T(8,128)(2,1)S(1)} %copy-done), kind=kOutput, calls=%fused_computation.76 | convolution fusion | flops 268435456 | bytes 8781824 | tf_op jit(solution)/shard_map/dot_general | solution.py:190
  253.9 4.5 %all-to-all-done.1 = f32[32,1,1024]{2,1,0:T(1,128)S(1)} async-done(((f32[32,1,1024]{2,1,0:T(1,128)}), f32[32,1,1024]{2,1,0:T(1,128)S(1)}, u32[]{:S(2)}, u32[]{:S(2)}) %all-to-all-start.1) | async-done | bytes 131104 | tf_op jit(solution)/shard_map/all_to_all | solution.py:18
  258.4 0.1 reduce_sum.47
  258.5 8.6 %add_convert_fusion = bf16[1024,2048]{1,0:T(8,128)(2,1)} fusion(f32[1024,2048]{1,0:T(8,128)} %fusion.61, f32[1024]{0:T(1024)S(1)} %mul.264, f32[1024]{0:T(1024)S(1)} %add_divide_fusion, bf16[256,1024]{1,0:T(8,128)(2,1)S(1)} %fusion.24, bf16[1,1024,2048]{2,1,0:T(8,128)(2,1)} %param.43, s32[1024]{0:T(1024)S(1)} %add_bitcast_fusion, ...), kind=kOutput, calls=%fused_computation | convolution fusion | flops 2156920832 | bytes 17314816 | tf_op jit(solution)/shard_map/dot_general | solution.py:186
  267.1 4.7 %copy.47 = bf16[16,2,32,2048]{3,2,0,1:T(8,128)(2,1)} copy(bf16[16,2,32,2048]{3,2,1,0:T(8,128)(2,1)} %bitcast.98) | data formatting | bytes 8388608 | tf_op jit(solution)/shard_map/reshape;reshape | solution.py:29
  271.8 0.1 reduce-scatter.3.cloned.1.call-update
  271.8 0.1 reduce-scatter.5.cloned.1.call-start
  271.9 15.7 %reduce-scatter.3.cloned.1.call-done = bf16[16,32,2048]{2,1,0:T(8,128)(2,1)} async-done(((bf16[32,32,2048]{2,1,0:T(8,128)(2,1)}), bf16[16,32,2048]{2,1,0:T(8,128)(2,1)}) %reduce-scatter.3.cloned.1.call-update) | async-done | bytes 2097168 | tf_op jit(solution)/shard_map/reduce_scatter | solution.py:33
  287.6 0.1 reduce-scatter.5.cloned.1.call-update
  287.6 73.5 %reduce-scatter.5.cloned.1.call-done = bf16[1,32,2048]{2,1,0:T(8,128)(2,1)} async-done(((bf16[16,32,2048]{2,1,0:T(8,128)(2,1)}), bf16[1,32,2048]{2,1,0:T(8,128)(2,1)}) %reduce-scatter.5.cloned.1.call-update) | async-done | bytes 131088 | tf_op jit(solution)/shard_map/reduce_scatter | solution.py:33
  361.2 1.6 fusion.42
  (41 shorter events, 0.2 us)
Async XLA Ops:
  7.2 242.2 %copy-start = (bf16[64,2048]{1,0:T(8,128)(2,1)S(1)}, bf16[64,2048]{1,0:T(8,128)(2,1)}, u32[]{:S(2)}) copy-start(bf16[64,2048]{1,0:T(8,128)(2,1)} %param.46) | copy-start | bytes 786436
  7.2 82.7 %copy-start.9 = (f32[2,64,16]{1,2,0:T(8,128)S(1)}, f32[2,64,16]{1,2,0:T(8,128)}, u32[]{:S(2)}) copy-start(f32[2,64,16]{1,2,0:T(8,128)} %param.35) | copy-start | bytes 24580
  7.2 83.0 %copy-start.8 = (f32[2,64,16]{1,2,0:T(8,128)S(1)}, f32[2,64,16]{1,2,0:T(8,128)}, u32[]{:S(2)}) copy-start(f32[2,64,16]{1,2,0:T(8,128)} %param.34) | copy-start | bytes 24580
  7.2 83.0 %copy-start.6 = (f32[1024,2,64]{0,2,1:T(8,128)S(1)}, f32[1024,2,64]{0,2,1:T(8,128)}, u32[]{:S(2)}) copy-start(f32[1024,2,64]{0,2,1:T(8,128)} %param.28) | copy-start | bytes 1572868
  7.2 83.0 %copy-start.5 = (f32[1024,2,64]{0,2,1:T(8,128)S(1)}, f32[1024,2,64]{0,2,1:T(8,128)}, u32[]{:S(2)}) copy-start(f32[1024,2,64]{0,2,1:T(8,128)} %param.27) | copy-start | bytes 1572868
  7.2 79.1 %all-gather.4.cloned.1.call-start = ((), (), s32[]{:S(2)}) async-start(), calls=%async_computation.5 | async-start | bytes 4325376 | tf_op jit(solution)/shard_map/all_gather | solution.py:147
  10.2 146.5 %all-gather.6.cloned.1.call-start = ((), (), s32[]{:S(2)}) async-start(), calls=%async_computation.6 | async-start | bytes 4325376 | tf_op jit(solution)/shard_map/all_gather | solution.py:162
  11.0 215.8 %all-gather.8.cloned.1.call-start = ((), (), s32[]{:S(2)}) async-start(), calls=%async_computation.7 | async-start | bytes 4325376 | tf_op jit(solution)/shard_map/all_gather | solution.py:169
  12.5 78.1 %copy-start.11 = (f32[2,16,64]{2,1,0:T(8,128)S(1)}, f32[2,16,64]{2,1,0:T(8,128)}, u32[]{:S(2)}) copy-start(f32[2,16,64]{2,1,0:T(8,128)} %param.36) | copy-start | bytes 24580
  12.5 78.3 %copy-start.10 = (f32[2,16,64]{2,1,0:T(8,128)S(1)}, f32[2,16,64]{2,1,0:T(8,128)}, u32[]{:S(2)}) copy-start(f32[2,16,64]{2,1,0:T(8,128)} %param.37) | copy-start | bytes 24580
  12.6 78.3 %copy-start.15 = (f32[2,16]{1,0:T(2,128)S(1)}, f32[2,16]{1,0:T(2,128)}, u32[]{:S(2)}) copy-start(f32[2,16]{1,0:T(2,128)} %param.38) | copy-start | bytes 388
  89.9 66.8 %copy-start.4 = (bf16[32,2048]{1,0:T(8,128)(2,1)S(1)}, bf16[32,2048]{1,0:T(8,128)(2,1)}, u32[]{:S(2)}) copy-start(bf16[32,2048]{1,0:T(8,128)(2,1)} %param.24) | copy-start | bytes 393220
  90.6 69.2 %copy-start.2 = (f32[1024,2,64]{0,2,1:T(8,128)}, f32[1024,2,64]{0,2,1:T(8,128)S(1)}, u32[]{:S(2)}) copy-start(f32[1024,2,64]{0,2,1:T(8,128)S(1)} %get-tuple-element.3) | copy-start | bytes 1572868
  90.6 69.2 %copy-start.3 = (f32[1024,2,64]{0,2,1:T(8,128)}, f32[1024,2,64]{0,2,1:T(8,128)S(1)}, u32[]{:S(2)}) copy-start(f32[1024,2,64]{0,2,1:T(8,128)S(1)} %get-tuple-element.4) | copy-start | bytes 1572868
  90.6 69.2 %copy-start.12 = (f32[2048]{0:T(1024)S(1)}, f32[2048]{0:T(1024)}, u32[]{:S(2)}) copy-start(f32[2048]{0:T(1024)} %param.40) | copy-start | bytes 24580
  90.8 69.9 %copy-start.13 = (f32[32,4]{0,1:T(4,128)S(1)}, f32[32,4]{0,1:T(4,128)}, u32[]{:S(2)}) copy-start(f32[32,4]{0,1:T(4,128)} %param.26) | copy-start | bytes 1540
  90.8 69.9 %copy-start.14 = (s32[32,4]{0,1:T(4,128)S(1)}, s32[32,4]{0,1:T(4,128)}, u32[]{:S(2)}) copy-start(s32[32,4]{0,1:T(4,128)} %param.25) | copy-start | bytes 1540
  90.9 135.9 %copy-start.7 = (bf16[2048,64]{0,1:T(8,128)(2,1)S(1)}, bf16[2048,64]{0,1:T(8,128)(2,1)}, u32[]{:S(2)}) copy-start(bf16[2048,64]{0,1:T(8,128)(2,1)} %param.44) | copy-start | bytes 786436
  159.9 70.6 %copy-start.19 = (bf16[2048,64]{0,1:T(8,128)(2,1)S(1)}, bf16[2048,64]{0,1:T(8,128)(2,1)}, u32[]{:S(2)}) copy-start(bf16[2048,64]{0,1:T(8,128)(2,1)} %param.45) | copy-start | bytes 786436
  226.8 3.7 %copy-start.1 = (bf16[1024,2048]{1,0:T(8,128)(2,1)S(1)}, bf16[1024,2048]{1,0:T(8,128)(2,1)}, u32[]{:S(2)}) copy-start(bf16[1024,2048]{1,0:T(8,128)(2,1)} %all-gather.8.cloned.1.call-done) | copy-start | bytes 12582916
  230.5 1.4 copy-start.16
  232.8 25.6 %all-to-all-start.1 = ((f32[32,1,1024]{2,1,0:T(1,128)}), f32[32,1,1024]{2,1,0:T(1,128)S(1)}, u32[]{:S(2)}, u32[]{:S(2)}) async-start(f32[32,1,1024]{2,1,0:T(1,128)} %broadcast_in_dim.10), calls=%async_computation.1 | async-start | bytes 262144 | tf_op jit(solution)/shard_map/all_to_all | solution.py:18
  241.9 45.7 %reduce-scatter.3.cloned.1.call-start = ((), (), s32[]{:S(2)}) async-start(), calls=%async_computation.8 | async-start | bytes 6291456 | tf_op jit(solution)/shard_map/reduce_scatter | solution.py:33
  242.1 3.6 copy-start.17
  245.7 2.2 copy-start.18
  271.8 89.3 %reduce-scatter.5.cloned.1.call-start = ((), (), s32[]{:S(2)}) async-start(), calls=%async_computation.9 | async-start | bytes 2228224 | tf_op jit(solution)/shard_map/reduce_scatter | solution.py:33
Sparse Core Ops, SparseCore 0:
  10.3 75.9 all-gather.3
  88.1 68.6 all-gather.5
  160.8 65.8 all-gather.7
  272.0 15.5 reduce-scatter.2
  289.8 71.2 reduce-scatter.4
where the time goes:
time: 370 us; the launch traced here: 369 us
  waiting for transfers between devices  255 us (69%)
  blocking collectives  42.7 us (12%)
  matrix products  32.3 us (9%)
  between operations  14.2 us (4%)
  starting transfers between devices  9.54 us (3%)
  local copies, waits for them, and re-layouts  8.9 us (2%)
  other arithmetic  6.62 us (2%)
    reduce_scatter x2, waiting for transfers between devices, reduced_to_own(): blocks = lax.psum_scatter(blocks, axes[k], scatter_dimension=0, tiled=True)  89.2 us
    all_gather x1, waiting for transfers between devices, on_device(): lax.all_gather(normed, EP, axis=0, tiled=True)  73.8 us
    all_gather x1, waiting for transfers between devices, on_device(): whole_rows = lax.all_gather(mixed, EP, axis=0, tiled=True)  45.6 us
    all_gather x1, waiting for transfers between devices, on_device(): whole_out = lax.all_gather(proj_out, EP, axis=0, tiled=True)  41.1 us
    all_to_all x1, blocking collectives, on_device(): lax.all_to_all(branch, EP, split_axis=0, concat_axis=1, tiled=True)  23.2 us
    all_to_all x1, blocking collectives, on_device(): lax.all_to_all(shares, EP, split_axis=1, concat_axis=0, tiled=True)[:, 0]  19.4 us
    all_to_all x1, starting transfers between devices, copy_for_each(): lax.all_to_all(jnp.broadcast_to(shard[None], (length, *shard.shape)), axi...  9.04 us
    dot_general x1, matrix products, on_device(): jnp.dot(selector.T, result, preferred_element_type=jnp.float32)  8.6 us
  transfers between devices with their start and end apart: 6, of which 6 were waited for; matrix products, arithmetic and copies ran while one was open for 5% of the time, Pallas kernels for 0%

commit v1 on v0

v1 whole, which is shorter than its diff:
```python
import functools

import jax
import jax.numpy as jnp
from jax import lax
from jax.experimental import pallas as pl
from jax.experimental.pallas import tpu as pltpu
from jax.sharding import PartitionSpec as P

EPS = 1e-06
LIMIT = 7.0
ALPHA = 1.702
MESH = pl.DeviceIdType.MESH
F32 = jnp.float32
BF16 = jnp.bfloat16
NT = (((1,), (1,)), ((), ()))


def dot(a, b):
    return jnp.dot(a, b, preferred_element_type=F32)


def dot_nt(a, b):
    return lax.dot_general(a, b, NT, preferred_element_type=F32)


def iota(shape, dim):
    return lax.broadcasted_iota(jnp.int32, shape, dim)


class Ring:
    def __init__(self, pieces, send, recv, where):
        self.pieces, self.send, self.recv, self.where = pieces, send, recv, where
        self.count = len(pieces)

    def copy(self, step, way, q):
        ref = self.pieces[q](self.where["block"](step, way))
        return pltpu.make_async_remote_copy(
            src_ref=ref,
            dst_ref=ref,
            send_sem=self.send.at[way, q],
            recv_sem=self.recv.at[way, step, q],
            device_id={"ep": self.where["next"][way]},
            device_id_type=MESH,
        )

    def arrival(self, step, way, q):
        ref = self.pieces[q](self.where["block"](step + 1, way))
        return pltpu.make_async_remote_copy(
            src_ref=ref,
            dst_ref=ref,
            send_sem=self.send.at[way, q],
            recv_sem=self.recv.at[way, step, q],
            device_id={"ep": self.where["next"][way]},
            device_id_type=MESH,
        )

    def half(self, way):
        mid = self.count // 2
        return range(mid) if way == 0 else range(mid, self.count)

    def first(self):
        for q in range(self.count):
            for way in (0, 1):
                self.copy(0, way, q).start()

    def piece(self, step, way, q, last=False):
        self.arrival(step - 1, way, q).wait_recv()
        self.copy(step - 1, way, q).wait_send()
        if not last or q in self.half(way):
            self.copy(step, way, q).start()

    def finish(self, hops):
        for way in (0, 1):
            for q in self.half(way):
                self.arrival(hops - 1, way, q).wait_recv()
                self.copy(hops - 1, way, q).wait_send()


def kernel(
    n,
    dims,
    tokens,
    routes_t,
    logits_t,
    state_re,
    state_im,
    gain_in,
    proj_in_t,
    params,
    in_re,
    in_im,
    out_re,
    out_im,
    proj_out,
    gain_mid,
    expert_gate,
    expert_up,
    expert_down,
    dense_gate_t,
    dense_up_t,
    dense_down,
    layer_out,
    new_re,
    new_im,
    rows_all,
    proj_all,
    branch_all,
    lhs_all,
    resid,
    own_res,
    mixed,
    w_gate,
    w_up,
    w_down,
    s_re,
    s_im,
    o_re,
    o_im,
    picked,
    active,
    down_rhs,
    combined,
    partner_part,
    ring_in,
    ring_out,
    units,
    pin4,
    dense_gu,
    hidden,
    logit_all,
    square,
    local_sem,
    out_sem,
    t_send,
    t_recv,
    p1_send,
    p1_recv,
    p2_send,
    p2_recv,
    b_send,
    b_recv,
    r_send,
    r_recv,
    td_send,
    td_recv,
    p1d_send,
    p1d_recv,
    p2d_send,
    p2d_recv,
    bd_send,
    bd_recv,
    cd_send,
    cd_recv,
    l_send,
    l_recv,
):
    rows, width, ff, cap = dims
    chips = n // 2
    hops = chips // 2
    seqs = n * rows
    block = seqs // 4
    per_block = n // 4
    slots = per_block * cap
    me = lax.axis_index("ep")
    chip = me // 2
    core = me % 2
    other = 1 - core
    partner = chip * 2 + other
    right = ((chip + 1) % chips) * 2 + core
    left = ((chip + chips - 1) % chips) * 2 + core
    nexts = (right, left)

    def block_of(step, way):
        at = (chip - step + chips) % chips if way == 0 else (chip + step) % chips
        return at * 2 + core

    where = {"next": nexts, "block": block_of}

    half_rows = rows // 2
    local = [
        pltpu.make_async_copy(tokens, rows_all.at[me, :, pl.ds(0, width)], local_sem.at[0]),
        pltpu.make_async_copy(proj_out, proj_all.at[me], local_sem.at[1]),
        pltpu.make_async_copy(state_re, s_re, local_sem.at[2]),
        pltpu.make_async_copy(state_im, s_im, local_sem.at[3]),
        pltpu.make_async_copy(expert_gate, w_gate, local_sem.at[4]),
        pltpu.make_async_copy(expert_up, w_up, local_sem.at[5]),
        pltpu.make_async_copy(expert_down, w_down, local_sem.at[6]),
    ]
    for i in range(4):
        local.append(pltpu.make_async_copy(proj_in_t, pin4.at[pl.ds(32 * i, 32)], local_sem.at[7 + i]))
        local.append(pltpu.make_async_copy(dense_down, down_rhs.at[i, pl.ds(0, 64)], local_sem.at[11 + i]))
    local.append(pltpu.make_async_copy(dense_gate_t, dense_gu.at[pl.ds(0, 64)], local_sem.at[15]))
    local.append(pltpu.make_async_copy(dense_up_t, dense_gu.at[pl.ds(64, 64)], local_sem.at[16]))
    for c in local:
        c.start()

    barrier = pltpu.get_barrier_semaphore()
    for peer in (left, right, partner):
        pl.semaphore_signal(barrier, inc=1, device_id={"ep": peer}, device_id_type=MESH)

    expert_row = iota((128, rows), 0)
    expert_id = expert_row % n
    scores = jnp.exp(logits_t[...])
    scores = scores / jnp.sum(scores, axis=0, keepdims=True)
    top = scores.shape[0]
    share = jnp.zeros((128, rows), F32)
    for k in range(top):
        share = share + jnp.where(routes_t[k : k + 1, :] == expert_id, scores[k : k + 1, :], 0.0)
    mark = jnp.where(share > 0.0, 1.0, 0.0)
    upper = jnp.where(iota((rows, rows), 0) <= iota((rows, rows), 1), 1.0, 0.0)
    rank = dot(mark.astype(BF16), upper.astype(BF16)) * mark
    part_hi = share.astype(BF16).astype(F32)
    kind = expert_row // n
    extra = jnp.where(
        kind == 0, part_hi, jnp.where(kind == 1, share - part_hi, jnp.where(kind == 2, rank, 0.0))
    )
    square[...] = jnp.zeros(square.shape, F32)
    square[:, 0:rows] = extra
    rows_all[me, :, width : width + 128] = square[...].T[0:rows, :].astype(BF16)

    pl.semaphore_wait(barrier, 3)

    ext = width + 128
    cut = ((ext // 128 + 1) // 2) * 128
    half_w = width // 2

    def row_piece(r0, c0, c1):
        return lambda dev: rows_all.at[dev, pl.ds(r0, half_rows), pl.ds(c0, c1 - c0)]

    def proj_piece(r0, c0):
        return lambda dev: proj_all.at[dev, pl.ds(r0, half_rows), pl.ds(c0, half_w)]

    def branch_piece(r0):
        return lambda dev: branch_all.at[dev, pl.ds(r0, block // 2)]

    t_ring = Ring(
        [
            row_piece(0, 0, cut),
            row_piece(0, cut, ext),
            row_piece(half_rows, 0, cut),
            row_piece(half_rows, cut, ext),
        ],
        t_send,
        t_recv,
        where,
    )
    p1_ring = Ring([proj_piece(0, 0), proj_piece(0, half_w)], p1_send, p1_recv, where)
    p2_ring = Ring([proj_piece(half_rows, 0), proj_piece(half_rows, half_w)], p2_send, p2_recv, where)
    b_ring = Ring([branch_piece(0), branch_piece(block // 2)], b_send, b_recv, where)

    class Share:
        def __init__(self, ref, send, recv):
            self.ref, self.send, self.recv = ref, send, recv

        def copy(self, dist, way, which):
            ref = self.ref(block_of(dist, way) // 2 * 2 + which)
            return pltpu.make_async_remote_copy(
                src_ref=ref,
                dst_ref=ref,
                send_sem=self.send.at[way],
                recv_sem=self.recv.at[way, dist],
                device_id={"ep": partner},
                device_id_type=MESH,
            )

        def give(self, dist, way, used=True):
            if used:
                self.copy(dist, way, core).wait_send()
            self.copy(dist, way, core).start()

        def take(self, dist, way):
            self.copy(dist, way, other).wait_recv()

        def close(self, dist):
            for way in (0, 1):
                self.copy(dist, way, core).wait_send()

    t_share = Share(lambda dev: rows_all.at[dev], td_send, td_recv)
    p1_share = Share(lambda dev: proj_all.at[dev, pl.ds(0, half_rows)], p1d_send, p1d_recv)
    p2_share = Share(lambda dev: proj_all.at[dev, pl.ds(half_rows, half_rows)], p2d_send, p2d_recv)
    b_share = Share(lambda dev: branch_all.at[dev], bd_send, bd_recv)

    local[0].wait()
    t_ring.first()
    t_share.give(0, 0, used=False)
    local[1].wait()
    p1_ring.first()
    p1_share.give(0, 0, used=False)
    for i in range(4):
        local[7 + 2 * i].wait()

    def unit_rows(dist, way):
        at = block_of(dist, way) // 2
        x = rows_all[pl.ds(at * 2, 2), :, 0:width].astype(F32).reshape(2 * rows, width)
        mean = jnp.sum(x * x, axis=-1, keepdims=True) * (1.0 / width)
        normed = (x * lax.rsqrt(mean + EPS) * gain_in[...]).astype(BF16)
        got = dot_nt(normed, pin4[...])
        spot = pl.multiple_of(at * (2 * rows), 2 * rows)
        units[pl.ds(spot, 2 * rows), :] = got.astype(BF16).astype(F32)

    def phase1(step, last=False):
        for q in range(t_ring.count):
            for way in (0, 1):
                t_ring.piece(step, way, q, last)
            if q % 2 == 1:
                for way in (0, 1):
                    p1_ring.piece(step, way, q // 2, last)

    def give1(dist, first=False):
        for way in (0, 1):
            t_share.give(dist, way, used=not (first and way == 1))
            p1_share.give(dist, way, used=not (first and way == 1))

    def take1(dist, ways=(0, 1)):
        for way in ways:
            t_share.take(dist, way)
            p1_share.take(dist, way)

    phase1(1, hops == 1)
    give1(1, first=True)
    take1(0, (0,))
    unit_rows(0, 0)

    def body1(step, carry):
        phase1(step)
        give1(step)
        take1(step - 1)
        unit_rows(step - 1, 0)
        unit_rows(step - 1, 1)
        return carry

    lax.fori_loop(2, hops - 1, body1, 0)
    phase1(hops - 1, True)
    give1(hops - 1)
    p2_ring.first()
    take1(hops - 2)
    unit_rows(hops - 2, 0)
    unit_rows(hops - 2, 1)
    take1(hops - 1)
    unit_rows(hops - 1, 0)
    unit_rows(hops - 1, 1)
    t_ring.finish(hops)
    p1_ring.finish(hops)
    t_share.give(hops, 0)
    p1_share.give(hops, 0)

    decay = -params[0:1, :]
    freq = params[1:2, :]
    step_size = jnp.exp(params[2:3, :])
    magnitude = jnp.exp(decay * step_size)
    carry_re = magnitude * jnp.cos(freq * step_size)
    carry_im = magnitude * jnp.sin(freq * step_size)
    denom = decay * decay + freq * freq
    feed_re = ((carry_re - 1.0) * decay + carry_im * freq) / denom
    feed_im = (carry_im * decay - (carry_re - 1.0) * freq) / denom
    same = (iota((32, 128), 0) // 16) == (iota((32, 128), 1) // 64)

    def spread(ref):
        return jnp.where(same, jnp.concatenate([ref[...], ref[...]], axis=1), 0.0)

    w_in_re, w_in_im = spread(in_re), spread(in_im)
    eff_re = feed_re * w_in_re - feed_im * w_in_im
    eff_im = feed_re * w_in_im + feed_im * w_in_re
    zeros = jnp.zeros((96, 128), F32)
    eff_re = jnp.concatenate([eff_re, zeros], axis=0).T.astype(BF16)
    eff_im = jnp.concatenate([eff_im, zeros], axis=0).T.astype(BF16)
    col_re = jnp.broadcast_to(carry_re, (128, 128)).T[:, 0:1]
    col_im = jnp.broadcast_to(carry_im, (128, 128)).T[:, 0:1]
    col_skip = jnp.broadcast_to(params[3:4, :], (128, 128)).T[:, 0:1]
    w_out = jnp.concatenate([spread(out_re), -spread(out_im)], axis=1)
    w_out = jnp.concatenate([w_out] * 4, axis=0).astype(BF16)

    t_share.take(hops, 0)
    p1_share.take(hops, 0)
    unit_rows(hops, 0)
    t_share.close(hops)
    p1_share.close(hops)
    local[2].wait()
    local[3].wait()

    lane_slot = iota((block, 128), 1) // 32
    packed = jnp.zeros((block, 128), F32)
    for r in range(4):
        at = slice(r * block, (r + 1) * block)
        u = units[at, :].T
        u16 = u.astype(BF16)
        old_re, old_im = s_re[:, at], s_im[:, at]
        fresh_re = col_re * old_re - col_im * old_im + dot(eff_re, u16)
        fresh_im = col_re * old_im + col_im * old_re + dot(eff_im, u16)
        o_re[:, at] = fresh_re
        o_im[:, at] = fresh_im
        both = jnp.concatenate([fresh_re, fresh_im], axis=0).astype(BF16)
        read = jax.nn.gelu(dot(w_out, both) + col_skip * u)
        packed = jnp.where(lane_slot == (r + me) % 4, read.T, packed)
    branch_all[me] = packed.astype(BF16)

    b_ring.first()
    b_share.give(0, 0, used=False)
    p2_share.give(0, 0, used=False)
    outs = [
        pltpu.make_async_copy(o_re, new_re, out_sem.at[0]),
        pltpu.make_async_copy(o_im, new_im, out_sem.at[1]),
    ]
    for c in outs:
        c.start()

    def phase2(step, last=False):
        for q in range(2):
            for way in (0, 1):
                p2_ring.piece(step, way, q, last)
            for way in (0, 1):
                b_ring.piece(step, way, q, last)

    def give2(dist, first=False):
        for way in (0, 1):
            b_share.give(dist, way, used=not (first and way == 1))
            p2_share.give(dist, way, used=not (first and way == 1))

    def take2(dist, ways=(0, 1)):
        for way in ways:
            b_share.take(dist, way)
            p2_share.take(dist, way)

    phase2(1, hops == 1)
    give2(1, first=True)
    take2(0, (0,))

    def body2(step, carry):
        phase2(step)
        give2(step)
        take2(step - 1)
        return carry

    lax.fori_loop(2, hops - 1, body2, 0)
    phase2(hops - 1, True)
    give2(hops - 1)
    take2(hops - 2)
    take2(hops - 1)
    p2_ring.finish(hops)
    b_ring.finish(hops)
    b_share.give(hops, 0)
    p2_share.give(hops, 0)
    b_share.take(hops, 0)
    p2_share.take(hops, 0)
    b_share.close(hops)
    p2_share.close(hops)

    for r in range(4):
        for k in range(n // 4):
            got = jnp.zeros((block, 128), F32)
            for i in range(4):
                got = jnp.where(lane_slot == (r + i) % 4, branch_all[4 * k + i].astype(F32), got)
            if r:
                got = pltpu.roll(got, 128 - 32 * r, 1)
            lhs_all[r * block : (r + 1) * block, 128 * k : 128 * k + 128] = got.astype(BF16)

    local[15].wait()
    local[16].wait()
    lane = iota((block, 128), 1)
    mix = params[4:5, :]
    mix_hi = mix.astype(BF16)
    mix_lo = (mix - mix_hi.astype(F32)).astype(BF16)
    mix_rows = jnp.where(
        iota((16, 128), 0) == 0,
        jnp.broadcast_to(mix_hi.astype(F32), (16, 128)),
        jnp.where(iota((16, 128), 0) == 1, jnp.broadcast_to(mix_lo.astype(F32), (16, 128)), 0.0),
    ).astype(BF16)
    wide = min(512, width)

    def mix_block(r, carry):
        base = pl.multiple_of(r * block, block)

        def part(j, c):
            cols = pl.ds(pl.multiple_of(j * wide, wide), wide)
            whole = proj_all[:, :, cols].reshape(n * 32, wide)
            x = rows_all[pl.ds(r * per_block, per_block), :, cols].astype(F32).reshape(block, wide)
            resid[:, cols] = x + dot(lhs_all[pl.ds(base, block), :], whole)
            return c

        lax.fori_loop(0, width // wide, part, 0)

        @pl.when(me // per_block == r)
        def _():
            own_res[...] = resid[pl.ds(pl.multiple_of((me % per_block) * rows, rows), rows), :]

        res = resid[...]
        mean = jnp.sum(res * res, axis=-1, keepdims=True) * (1.0 / width)
        m16 = (res * lax.rsqrt(mean + EPS) * gain_mid[...]).astype(BF16)
        mixed[pl.ds(base, block), :] = m16
        gu = dot_nt(m16, dense_gu[...])
        hid = jnp.where(lane < 64, jax.nn.silu(gu) * pltpu.roll(gu, 64, 1), 0.0).astype(BF16)
        hidden[pl.ds(base, block), :] = hid
        row = jnp.sum(dot_nt(mix_rows, hid), axis=0, keepdims=True)
        logit_all[me, :, pl.ds(base, block)] = row
        return carry

    lax.fori_loop(0, 4, mix_block, 0)

    def logit_copy(j):
        to = (me + j) % n
        return pltpu.make_async_remote_copy(
            src_ref=logit_all.at[me],
            dst_ref=logit_all.at[me],
            send_sem=l_send.at[j],
            recv_sem=l_recv.at[j],
            device_id={"ep": to},
            device_id_type=MESH,
        )

    def logit_arrival(j):
        source = (me - j + n) % n
        return pltpu.make_async_remote_copy(
            src_ref=logit_all.at[source],
            dst_ref=logit_all.at[source],
            send_sem=l_send.at[j],
            recv_sem=l_recv.at[j],
            device_id={"ep": source},
            device_id_type=MESH,
        )

    def send_logit(j, carry):
        logit_copy(j).start()
        return carry

    lax.fori_loop(1, n, send_logit, 0)

    def chosen(r):
        extra = rows_all[pl.ds(r * per_block, per_block), :, width : width + 128]
        extra = extra.astype(F32).reshape(block, 128)
        weight = jnp.sum(
            jnp.where((lane == me) | (lane == n + me), extra, 0.0), axis=-1, keepdims=True
        )
        spot = jnp.sum(jnp.where(lane == 2 * n + me, extra, 0.0), axis=-1, keepdims=True)
        source = (iota((block, 1), 0) // rows).astype(F32)
        slot = jnp.where(spot > 0.5, source * cap + spot - 1.0, -1.0)
        return weight, slot

    lane_f = lane.astype(F32)
    for r in range(4):
        _, slot = chosen(r)
        hot = jnp.where(lane_f == slot, 1.0, 0.0).T.astype(BF16)
        picked[r * slots : (r + 1) * slots, :] = dot(
            hot[0:slots, :], mixed[r * block : (r + 1) * block, :]
        ).astype(BF16)
    local[4].wait()
    local[5].wait()
    local[6].wait()
    fcut = min(256, ff)

    def up_part(j, carry):
        cols = pl.ds(pl.multiple_of(j * fcut, fcut), fcut)
        gated = jnp.minimum(dot(picked[...], w_gate[:, cols]), LIMIT)
        up = jnp.clip(dot(picked[...], w_up[:, cols]), -LIMIT, LIMIT)
        active[:, cols] = ((up + 1.0) * gated * jax.nn.sigmoid(ALPHA * gated)).astype(BF16)
        return carry

    lax.fori_loop(0, ff // fcut, up_part, 0)
    for i in range(4):
        local[8 + 2 * i].wait()

    def down_part(j, carry):
        cols = pl.ds(pl.multiple_of(j * wide, wide), wide)
        out = dot(active[...], w_down[:, cols]).astype(BF16)
        for r in range(4):
            down_rhs[r, 64 : 64 + slots, cols] = out[r * slots : (r + 1) * slots, :]
        return carry

    lax.fori_loop(0, width // wide, down_part, 0)

    def take_logit(j, carry):
        logit_arrival(j).wait_recv()
        logit_copy(j).wait_send()
        return carry

    lax.fori_loop(1, n, take_logit, 0)
    gate_row = jax.nn.sigmoid(jnp.sum(logit_all[...], axis=0))

    def hand_over(r):
        ref = combined.at[other, pl.ds(r * (chips // 4), chips // 4)]
        return pltpu.make_async_remote_copy(
            src_ref=ref,
            dst_ref=partner_part.at[pl.ds(r * (chips // 4), chips // 4)],
            send_sem=cd_send.at[r],
            recv_sem=cd_recv.at[r],
            device_id={"ep": partner},
            device_id_type=MESH,
        )

    for r in range(4):
        at = slice(r * block, (r + 1) * block)
        gate = jnp.broadcast_to(gate_row[:, at], (128, block)).T
        weight, slot = chosen(r)
        lhs = jnp.where(
            lane < 64,
            gate * hidden[at, :].astype(F32),
            jnp.where(lane_f == slot + 64.0, jnp.where(slot >= 0.0, weight, 0.0), 0.0),
        )
        lhs = lhs[:, 0 : 64 + slots].astype(BF16)

        def spread_part(j, carry, r=r, lhs=lhs):
            cols = pl.ds(pl.multiple_of(j * wide, wide), wide)
            out = dot(lhs, down_rhs[r, :, cols]).astype(BF16)
            out = out.reshape(per_block // 2, 2, rows, wide)
            for c in range(2):
                combined[c, pl.ds(r * (chips // 4), chips // 4), :, cols] = out[:, c]
            return carry

        lax.fori_loop(0, width // wide, spread_part, 0)
        hand_over(r).start()

    for r in range(4):
        hand_over(r).wait_recv()

    pieces = [(a, b) for a in range(2) for b in range(2)]

    def rs_copy(step, way, q):
        a, b = pieces[q]
        return pltpu.make_async_remote_copy(
            src_ref=ring_out.at[way, step, pl.ds(a * half_rows, half_rows), pl.ds(b * half_w, half_w)],
            dst_ref=ring_in.at[way, step, pl.ds(a * half_rows, half_rows), pl.ds(b * half_w, half_w)],
            send_sem=r_send.at[way, q],
            recv_sem=r_recv.at[way, step, q],
            device_id={"ep": nexts[way]},
            device_id_type=MESH,
        )

    def rs_own(dist, way, q):
        a, b = pieces[q]
        to = (chip + dist) % chips if way == 0 else (chip - dist + chips) % chips
        rr, cc = pl.ds(a * half_rows, half_rows), pl.ds(b * half_w, half_w)
        return combined[core, to, rr, cc].astype(F32) + partner_part[to, rr, cc].astype(F32)

    def rs_step(step, way, q, got, used):
        a, b = pieces[q]
        rr, cc = pl.ds(a * half_rows, half_rows), pl.ds(b * half_w, half_w)
        value = rs_own(hops - step, way, q)
        if got:
            rs_copy(step - 1, way, q).wait_recv()
            value = value + ring_in[way, step - 1, rr, cc].astype(F32)
        if used:
            rs_copy(step - 1, way, q).wait_send()
        ring_out[way, step, rr, cc] = value.astype(BF16)
        rs_copy(step, way, q).start()

    halves = (range(0, 2), range(2, 4))
    for i in range(2):
        for way in (0, 1):
            rs_step(0, way, halves[way][i], False, False)
    for i in range(2):
        for way in (0, 1):
            rs_step(1, way, halves[1 - way][i], False, False)
    for i in range(2):
        for way in (0, 1):
            rs_step(1, way, halves[way][i], True, True)

    def rs_body(step, carry):
        for q in range(4):
            for way in (0, 1):
                rs_step(step, way, q, True, True)
        return carry

    lax.fori_loop(2, hops, rs_body, 0)
    for q in range(4):
        a, b = pieces[q]
        rr, cc = pl.ds(a * half_rows, half_rows), pl.ds(b * half_w, half_w)
        value = rs_own(0, 0, q) + own_res[rr, cc]
        for way in (0, 1):
            rs_copy(hops - 1, way, q).wait_recv()
            value = value + ring_in[way, hops - 1, rr, cc].astype(F32)
        layer_out[rr, cc] = value.astype(BF16)
    for q in range(4):
        for way in (0, 1):
            rs_copy(hops - 1, way, q).wait_send()
    for r in range(4):
        hand_over(r).wait_send()
    for c in outs:
        c.wait()


def on_device(
    tokens,
    routes,
    route_logits,
    state_real,
    state_imag,
    gain_in,
    proj_in,
    decay_rate,
    frequency,
    log_step,
    input_real,
    input_imag,
    output_real,
    output_imag,
    skip_gain,
    proj_out,
    gain_mid,
    expert_gate,
    expert_up,
    expert_down,
    dense_gate,
    dense_up,
    dense_down,
    dense_mix,
):
    n = lax.axis_size("ep")
    rows, width = tokens.shape
    top = routes.shape[1]
    ff = expert_gate.shape[2]
    seqs = state_real.shape[0]
    cap = max(2, 2 * rows * top // n)
    chips, hops, block = n // 2, n // 4, seqs // 4
    slots = (n // 4) * cap
    params = jnp.stack(
        [
            decay_rate.reshape(128),
            frequency.reshape(128),
            jnp.repeat(log_step, 64),
            jnp.tile(skip_gain.reshape(32), 4),
            jnp.pad(dense_mix, (0, 64)),
        ]
    )
    operands = (
        tokens,
        routes.T,
        route_logits.T,
        state_real.transpose(1, 2, 0).reshape(128, seqs),
        state_imag.transpose(1, 2, 0).reshape(128, seqs),
        gain_in[None],
        proj_in.T,
        params,
        input_real.transpose(0, 2, 1).reshape(32, 64),
        input_imag.transpose(0, 2, 1).reshape(32, 64),
        output_real.reshape(32, 64),
        output_imag.reshape(32, 64),
        proj_out,
        gain_mid[None],
        expert_gate[0],
        expert_up[0],
        expert_down[0],
        dense_gate.T,
        dense_up.T,
        dense_down,
    )
    vmem = pl.BlockSpec(memory_space=pltpu.VMEM)
    far = pl.BlockSpec(memory_space=pl.ANY)
    in_specs = [
        far,
        vmem,
        vmem,
        far,
        far,
        vmem,
        far,
        vmem,
        vmem,
        vmem,
        vmem,
        vmem,
        far,
        vmem,
        far,
        far,
        far,
        far,
        far,
        far,
    ]
    V = pltpu.VMEM
    dma = pltpu.SemaphoreType.DMA
    scratch = [
        V((n, rows, width + 128), BF16),
        V((n, 32, width), BF16),
        V((n, block, 128), BF16),
        V((seqs, n * 32), BF16),
        V((block, width), F32),
        V((rows, width), F32),
        V((seqs, width), BF16),
        V((width, ff), BF16),
        V((width, ff), BF16),
        V((ff, width), BF16),
        V((128, seqs), F32),
        V((128, seqs), F32),
        V((128, seqs), F32),
        V((128, seqs), F32),
        V((4 * slots, width), BF16),
        V((4 * slots, ff), BF16),
        V((4, 64 + slots, width), BF16),
        V((2, chips, rows, width), BF16),
        V((chips, rows, width), BF16),
        V((2, hops, rows, width), BF16),
        V((2, hops, rows, width), BF16),
        V((seqs, 128), F32),
        V((128, width), BF16),
        V((128, width), BF16),
        V((seqs, 128), BF16),
        V((n, 1, seqs), F32),
        V((128, 128), F32),
        dma((17,)),
        dma((2,)),
        dma((2, 4)),
        dma((2, hops, 4)),
        dma((2, 2)),
        dma((2, hops, 2)),
        dma((2, 2)),
        dma((2, hops, 2)),
        dma((2, 2)),
        dma((2, hops, 2)),
        dma((2, 4)),
        dma((2, hops, 4)),
    ]
    for _ in range(4):
        scratch += [dma((2,)), dma((2, hops + 1))]
    scratch += [dma((4,)), dma((4,)), dma((n,)), dma((n,))]
    layer_out, new_re, new_im = pl.pallas_call(
        functools.partial(kernel, n, (rows, width, ff, cap)),
        out_shape=(
            jax.ShapeDtypeStruct((rows, width), BF16),
            jax.ShapeDtypeStruct((128, seqs), F32),
            jax.ShapeDtypeStruct((128, seqs), F32),
        ),
        in_specs=in_specs,
        out_specs=(vmem, far, far),
        scratch_shapes=scratch,
        compiler_params=pltpu.CompilerParams(
            collective_id=0, has_side_effects=True, vmem_limit_bytes=66_000_000
        ),
        name="layer_step",
    )(*operands)
    groups, state = state_real.shape[1:]

    def back(values):
        return values.reshape(groups, state, seqs).transpose(2, 0, 1)

    return (layer_out, back(new_re), back(new_im))


def solution(mesh):
    both = ("grp", "ep")
    return jax.shard_map(
        on_device,
        mesh=mesh,
        in_specs=(
            P(both, None),
            P(both, None),
            P(both, None),
            P("grp", "ep", None),
            P("grp", "ep", None),
            P(),
            P(None, "ep"),
            P("ep", None),
            P("ep", None),
            P("ep"),
            P("ep", None, None),
            P("ep", None, None),
            P("ep", None, None),
            P("ep", None, None),
            P("ep", None),
            P("ep", None),
            P(),
            P("ep", None, None),
            P("ep", None, None),
            P("ep", None, None),
            P(None, "ep"),
            P(None, "ep"),
            P("ep", None),
            P("ep"),
        ),
        out_specs=(P(both, None), P("grp", "ep", None), P("grp", "ep", None)),
        check_vma=False,
    )
```

time: 370 us -> 155 us (0.42)
  waiting for transfers between devices: 255 us -> 0 us
  Pallas kernels: 0 us -> 144 us
  blocking collectives: 42.7 us -> 0 us
  matrix products: 32.3 us -> 0 us
  between operations: 14.2 us -> 0.64 us
  starting transfers between devices: 9.54 us -> 0 us
  other arithmetic: 6.62 us -> 0 us
    all_gather x3 -> x0, waiting for transfers between devices: 160 us -> none  [the longest x1 73.8 us: on_device(): lax.all_gather(normed, EP, axis=0, tiled=True)]
    pallas_call x0 -> x1, Pallas kernels: none -> 144 us  [on_device(): pl.pallas_call(functools.partial(kernel, n, (rows, width, ff, cap)), out_...]
    reduce_scatter x2 -> x0, waiting for transfers between devices: 89.2 us -> none  [reduced_to_own(): blocks = lax.psum_scatter(blocks, axes[k], scatter_dimension=0, tiled=True)]
    all_to_all x2 -> x0, blocking collectives: 42.7 us -> none  [the longest x1 23.2 us: on_device(): lax.all_to_all(branch, EP, split_axis=0, concat_axis=1, tiled=True)]
    dot_general x14 -> x0, matrix products: 32.3 us -> none  [the longest x1 8.6 us: on_device(): jnp.dot(selector.T, result, preferred_element_type=jnp.float32)]
    all_to_all x1 -> x0, starting transfers between devices: 9.04 us -> none  [copy_for_each(): lax.all_to_all(jnp.broadcast_to(shard[None], (length, *shard.shape)), axi...]
    all_to_all x1 -> x0, waiting for transfers between devices: 4.5 us -> none  [copy_for_each(): lax.all_to_all(jnp.broadcast_to(shard[None], (length, *shard.shape)), axi...]
    convert_element_type x4 -> x0, other arithmetic: 4.05 us -> none  [the longest x1 1.67 us: on_device(): normed = rms_scale(inputs, gain_in).astype(jnp.bfloat16)]
  transfers between devices with their start and end apart: 6 -> 0, of which waited for: 6 -> 0; matrix products, arithmetic and copies ran while one was open for 5% -> 0% of each run, Pallas kernels for 0% -> 0%
where the time goes in v1:
time: 155 us; the launch traced here: 154 us
  Pallas kernels  144 us (93%)
  local copies, waits for them, and re-layouts  9.77 us (6%)
    pallas_call x1, Pallas kernels, on_device(): pl.pallas_call(functools.partial(kernel, n, (rows, width, ff, cap)), out_...  144 us
    unnamed x3, local copies, waits for them, and re-layouts  5.34 us

profile of v1, /device:TPU:86, one launch (start us, length us, event | category | flops | bytes accessed | tf_op | source)
XLA Modules:
  0.0 154.2 jit_solution(2621396253388161197)
XLA Ops:
  0.6 0.8 stack_reshape.9
  1.4 0.8 stack_reshape.10
  2.1 0.8 tile.7
  2.9 0.7 pad_bitcast_fusion
  3.6 0.7 broadcast_in_dim.10
  4.3 0.1 stack_reshape.11
  4.4 0.1 stack_tile.3
  4.5 0.6 stack.7.params
  5.1 143.8 %layer_step.1 = (bf16[32,2048]{1,0:T(8,128)(2,1)}, f32[128,1024]{1,0:T(8,128)}, f32[128,1024]{1,0:T(8,128)}) custom-call(bf16[32,2048]{1,0:T(8,128)(2,1)} %tokens.1, s32[4,32]{1,0:T(4,128)} %bitcast.48, f32[4,32]{1,0:T(4,128)} %bitcast.49, f32[128,1024]{1,0:T(8,128)} %bitcast.35, f32[128,1024]{1,0:T(8,128)} %bitcast.36, f32[1,2048]{1,0:T(1,128)} %bitcast.46, ...), custom_call_target="tpu_custom_call" | custom-call | tf_op jit(solution)/shard_map/layer_step/pallas_call | solution.py:816
  148.9 1.6 %copy.30 = bf16[32,2048]{1,0:T(8,128)(2,1)} copy(bf16[32,2048]{1,0:T(8,128)(2,1)} %get-tuple-element.12) | data formatting | bytes 262144
  150.5 1.9 %copy.31 = f32[1024,2,64]{0,2,1:T(8,128)} copy(f32[1024,2,64]{0,2,1:T(8,128)} %bitcast.38) | data formatting | bytes 1048576
  152.3 1.9 %copy.32 = f32[1024,2,64]{0,2,1:T(8,128)} copy(f32[1024,2,64]{0,2,1:T(8,128)} %bitcast.37) | data formatting | bytes 1048576
  (1 shorter events, 0.0 us)

commit v2 on v1

--- a/solution.py
+++ b/solution.py
@@ -87,7 +87,11 @@
     state_im,
     gain_in,
     proj_in_t,
-    params,
+    decay_rate,
+    frequency,
+    log_step,
+    skip_gain,
+    dense_mix,
     in_re,
     in_im,
     out_re,
@@ -106,9 +110,7 @@
     rows_all,
     proj_all,
     branch_all,
-    lhs_all,
-    resid,
-    own_res,
+    total,
     mixed,
     w_gate,
     w_up,
@@ -118,6 +120,7 @@
     o_re,
     o_im,
     picked,
+    final_lhs,
     active,
     down_rhs,
     combined,
@@ -127,33 +130,32 @@
     units,
     pin4,
     dense_gu,
-    hidden,
+    spread_lhs,
+    scale_all,
+    logit_pair,
     logit_all,
     square,
     local_sem,
     out_sem,
     t_send,
-    t_recv,
     p1_send,
-    p1_recv,
     p2_send,
-    p2_recv,
     b_send,
-    b_recv,
     r_send,
-    r_recv,
+    recv_a,
+    recv_b,
     td_send,
-    td_recv,
     p1d_send,
-    p1d_recv,
     p2d_send,
-    p2d_recv,
     bd_send,
-    bd_recv,
+    share_a,
+    share_b,
     cd_send,
     cd_recv,
     l_send,
     l_recv,
+    lp_send,
+    lp_recv,
 ):
     rows, width, ff, cap = dims
     chips = n // 2
@@ -192,8 +194,8 @@
         local.append(pltpu.make_async_copy(dense_down, down_rhs.at[i, pl.ds(0, 64)], local_sem.at[11 + i]))
     local.append(pltpu.make_async_copy(dense_gate_t, dense_gu.at[pl.ds(0, 64)], local_sem.at[15]))
     local.append(pltpu.make_async_copy(dense_up_t, dense_gu.at[pl.ds(64, 64)], local_sem.at[16]))
-    for c in local:
-        c.start()
+    for i in (0, 1, 7, 9, 11, 13):
+        local[i].start()
 
     barrier = pltpu.get_barrier_semaphore()
     for peer in (left, right, partner):
@@ -228,11 +230,11 @@
     def row_piece(r0, c0, c1):
         return lambda dev: rows_all.at[dev, pl.ds(r0, half_rows), pl.ds(c0, c1 - c0)]
 
-    def proj_piece(r0, c0):
-        return lambda dev: proj_all.at[dev, pl.ds(r0, half_rows), pl.ds(c0, half_w)]
+    def proj_piece(r0, c0, size):
+        return lambda dev: proj_all.at[dev, pl.ds(r0, half_rows), pl.ds(c0, size)]
 
     def branch_piece(r0):
-        return lambda dev: branch_all.at[dev, pl.ds(r0, block // 2)]
+        return lambda dev: branch_all.at[dev, pl.ds(r0, block // 4)]
 
     t_ring = Ring(
         [
@@ -242,12 +244,14 @@
             row_piece(half_rows, cut, ext),
         ],
         t_send,
-        t_recv,
+        recv_a,
         where,
     )
-    p1_ring = Ring([proj_piece(0, 0), proj_piece(0, half_w)], p1_send, p1_recv, where)
-    p2_ring = Ring([proj_piece(half_rows, 0), proj_piece(half_rows, half_w)], p2_send, p2_recv, where)
-    b_ring = Ring([branch_piece(0), branch_piece(block // 2)], b_send, b_recv, where)
+    p1_ring = Ring([proj_piece(0, 0, half_w), proj_piece(0, half_w, half_w)], p1_send, recv_b, where)
+    p2_ring = Ring(
+        [proj_piece(half_rows, i * (width // 4), width // 4) for i in range(4)], p2_send, recv_b, where
+    )
+    b_ring = Ring([branch_piece(i * (block // 4)) for i in range(4)], b_send, recv_a, where)
 
     class Share:
         def __init__(self, ref, send, recv):
@@ -276,10 +280,10 @@
             for way in (0, 1):
                 self.copy(dist, way, core).wait_send()
 
-    t_share = Share(lambda dev: rows_all.at[dev], td_send, td_recv)
-    p1_share = Share(lambda dev: proj_all.at[dev, pl.ds(0, half_rows)], p1d_send, p1d_recv)
-    p2_share = Share(lambda dev: proj_all.at[dev, pl.ds(half_rows, half_rows)], p2d_send, p2d_recv)
-    b_share = Share(lambda dev: branch_all.at[dev], bd_send, bd_recv)
+    t_share = Share(lambda dev: rows_all.at[dev], td_send, share_a)
+    p1_share = Share(lambda dev: proj_all.at[dev, pl.ds(0, half_rows)], p1d_send, share_b)
+    p2_share = Share(lambda dev: proj_all.at[dev, pl.ds(half_rows, half_rows)], p2d_send, share_b)
+    b_share = Share(lambda dev: branch_all.at[dev], bd_send, share_a)
 
     local[0].wait()
     t_ring.first()
@@ -287,6 +291,9 @@
     local[1].wait()
     p1_ring.first()
     p1_share.give(0, 0, used=False)
+    for i in range(17):
+        if i not in (0, 1, 7, 9, 11, 13):
+            local[i].start()
     for i in range(4):
         local[7 + 2 * i].wait()
 
@@ -297,6 +304,7 @@
         normed = (x * lax.rsqrt(mean + EPS) * gain_in[...]).astype(BF16)
         got = dot_nt(normed, pin4[...])
         spot = pl.multiple_of(at * (2 * rows), 2 * rows)
+        total[pl.ds(spot, 2 * rows), :] = x
         units[pl.ds(spot, 2 * rows), :] = got.astype(BF16).astype(F32)
 
     def phase1(step, last=False):
@@ -334,6 +342,7 @@
     phase1(hops - 1, True)
     give1(hops - 1)
     p2_ring.first()
+    p2_share.give(0, 0, used=False)
     take1(hops - 2)
     unit_rows(hops - 2, 0)
     unit_rows(hops - 2, 1)
@@ -345,9 +354,12 @@
     t_share.give(hops, 0)
     p1_share.give(hops, 0)
 
-    decay = -params[0:1, :]
-    freq = params[1:2, :]
-    step_size = jnp.exp(params[2:3, :])
+    def flat(ref):
+        return jnp.concatenate([ref[0:1, :], ref[1:2, :]], axis=1)
+
+    decay = -flat(decay_rate)
+    freq = flat(frequency)
+    step_size = jnp.exp(jnp.where(iota((1, 128), 1) < 64, log_step[0:1, 0:1], log_step[0:1, 1:2]))
     magnitude = jnp.exp(decay * step_size)
     carry_re = magnitude * jnp.cos(freq * step_size)
     carry_im = magnitude * jnp.sin(freq * step_size)
@@ -367,7 +379,11 @@
     eff_im = jnp.concatenate([eff_im, zeros], axis=0).T.astype(BF16)
     col_re = jnp.broadcast_to(carry_re, (128, 128)).T[:, 0:1]
     col_im = jnp.broadcast_to(carry_im, (128, 128)).T[:, 0:1]
-    col_skip = jnp.broadcast_to(params[3:4, :], (128, 128)).T[:, 0:1]
+    skip_row = iota((128, 16), 0) % 32
+    skips = jnp.where(skip_row < 16, skip_gain[0:1, :], skip_gain[1:2, :])
+    col_skip = jnp.sum(
+        jnp.where(skip_row % 16 == iota((128, 16), 1), skips, 0.0), axis=1, keepdims=True
+    )
     w_out = jnp.concatenate([spread(out_re), -spread(out_im)], axis=1)
     w_out = jnp.concatenate([w_out] * 4, axis=0).astype(BF16)
 
@@ -379,6 +395,14 @@
     local[2].wait()
     local[3].wait()
 
+    def p2_step(step, last=False):
+        for q in range(4):
+            for way in (0, 1):
+                p2_ring.piece(step, way, q, last)
+        p2_share.give(step, 0)
+        p2_share.give(step, 1, used=step > 1) if isinstance(step, int) else p2_share.give(step, 1)
+
+    p2_step(1)
     lane_slot = iota((block, 128), 1) // 32
     packed = jnp.zeros((block, 128), F32)
     for r in range(4):
@@ -397,7 +421,6 @@
 
     b_ring.first()
     b_share.give(0, 0, used=False)
-    p2_share.give(0, 0, used=False)
     outs = [
         pltpu.make_async_copy(o_re, new_re, out_sem.at[0]),
         pltpu.make_async_copy(o_im, new_im, out_sem.at[1]),
@@ -405,117 +428,144 @@
     for c in outs:
         c.start()
 
-    def phase2(step, last=False):
-        for q in range(2):
-            for way in (0, 1):
-                p2_ring.piece(step, way, q, last)
-            for way in (0, 1):
-                b_ring.piece(step, way, q, last)
-
-    def give2(dist, first=False):
-        for way in (0, 1):
-            b_share.give(dist, way, used=not (first and way == 1))
-            p2_share.give(dist, way, used=not (first and way == 1))
-
-    def take2(dist, ways=(0, 1)):
-        for way in ways:
+    wide = min(512, width)
+
+    def pair_of(k):
+        a, b = block_of(k, 0) // 2, block_of(k + 1, 1) // 2
+        even = jnp.where(a % 2 == 0, a, b)
+        return even, a + b - even
+
+    def pair_lhs(k, r):
+        even, odd = pair_of(k)
+        got = branch_all[2 * even].astype(F32)
+        for i, dev in ((1, 2 * even + 1), (2, 2 * odd), (3, 2 * odd + 1)):
+            got = jnp.where(lane_slot == (r + i) % 4, branch_all[dev].astype(F32), got)
+        return pltpu.roll(got, (128 - 32 * r) % 128, 1).astype(BF16)
+
+    def quad_lhs(j, r):
+        return jnp.concatenate([pair_lhs(2 * j, r), pair_lhs(2 * j + 1, r)], axis=1)
+
+    def quad_rhs(j, cols):
+        chips4 = pair_of(2 * j) + pair_of(2 * j + 1)
+        return jnp.concatenate(
+            [proj_all[pl.ds(2 * at, 2), :, cols].reshape(64, wide) for at in chips4], axis=0
+        )
+
+    def mix_rows(j, r):
+        at = pl.ds(pl.multiple_of(r * block, block), block)
+        lhs = quad_lhs(j, r)
+        for c in range(width // wide):
+            cols = slice(c * wide, (c + 1) * wide)
+            total[at, cols] = total[at, cols] + dot(lhs, quad_rhs(j, cols))
+
+    def take2(dist):
+        for way in (0,) if isinstance(dist, int) and dist in (0, hops) else (0, 1):
             b_share.take(dist, way)
             p2_share.take(dist, way)
 
-    phase2(1, hops == 1)
-    give2(1, first=True)
-    take2(0, (0,))
+    def b_step(step, p2_next, last=False, p2_last=False):
+        for q in range(4):
+            for way in (0, 1):
+                if p2_next is not None:
+                    p2_ring.piece(p2_next, way, q, p2_last)
+                b_ring.piece(step, way, q, last)
+            if isinstance(step, int) and step < 3:
+                continue
+            if q == 0:
+                take2(step - 1)
+            if q % 2 == 1:
+                turn = step - 3
+                mix_rows(turn // 2, turn % 2 * 2 + q // 2)
+        first = isinstance(step, int) and step == 1
+        for way in (0, 1):
+            if p2_next is not None:
+                p2_share.give(p2_next, way)
+            b_share.give(step, way, used=not (first and way == 1))
+
+    b_step(1, 2)
+    take2(0)
+    b_step(2, 3, p2_last=hops == 4)
+    take2(1)
 
     def body2(step, carry):
-        phase2(step)
-        give2(step)
-        take2(step - 1)
+        b_step(step, step + 1)
         return carry
 
-    lax.fori_loop(2, hops - 1, body2, 0)
-    phase2(hops - 1, True)
-    give2(hops - 1)
-    take2(hops - 2)
+    lax.fori_loop(3, hops - 2, body2, 0)
+    if hops > 4:
+        b_step(hops - 2, hops - 1, p2_last=True)
+    b_step(hops - 1, None, last=True)
+    p2_ring.finish(hops)
+    p2_share.give(hops, 0)
     take2(hops - 1)
-    p2_ring.finish(hops)
+    mix_rows(hops // 2 - 2, 2)
+    mix_rows(hops // 2 - 2, 3)
     b_ring.finish(hops)
     b_share.give(hops, 0)
-    p2_share.give(hops, 0)
-    b_share.take(hops, 0)
-    p2_share.take(hops, 0)
+    take2(hops)
     b_share.close(hops)
     p2_share.close(hops)
-
-    for r in range(4):
-        for k in range(n // 4):
-            got = jnp.zeros((block, 128), F32)
-            for i in range(4):
-                got = jnp.where(lane_slot == (r + i) % 4, branch_all[4 * k + i].astype(F32), got)
-            if r:
-                got = pltpu.roll(got, 128 - 32 * r, 1)
-            lhs_all[r * block : (r + 1) * block, 128 * k : 128 * k + 128] = got.astype(BF16)
 
     local[15].wait()
     local[16].wait()
     lane = iota((block, 128), 1)
-    mix = params[4:5, :]
-    mix_hi = mix.astype(BF16)
-    mix_lo = (mix - mix_hi.astype(F32)).astype(BF16)
-    mix_rows = jnp.where(
-        iota((16, 128), 0) == 0,
-        jnp.broadcast_to(mix_hi.astype(F32), (16, 128)),
-        jnp.where(iota((16, 128), 0) == 1, jnp.broadcast_to(mix_lo.astype(F32), (16, 128)), 0.0),
-    ).astype(BF16)
-    wide = min(512, width)
-
-    def mix_block(r, carry):
-        base = pl.multiple_of(r * block, block)
-
-        def part(j, c):
-            cols = pl.ds(pl.multiple_of(j * wide, wide), wide)
-            whole = proj_all[:, :, cols].reshape(n * 32, wide)
-            x = rows_all[pl.ds(r * per_block, per_block), :, cols].astype(F32).reshape(block, wide)
-            resid[:, cols] = x + dot(lhs_all[pl.ds(base, block), :], whole)
-            return c
-
-        lax.fori_loop(0, width // wide, part, 0)
-
-        @pl.when(me // per_block == r)
-        def _():
-            own_res[...] = resid[pl.ds(pl.multiple_of((me % per_block) * rows, rows), rows), :]
-
-        res = resid[...]
-        mean = jnp.sum(res * res, axis=-1, keepdims=True) * (1.0 / width)
-        m16 = (res * lax.rsqrt(mean + EPS) * gain_mid[...]).astype(BF16)
-        mixed[pl.ds(base, block), :] = m16
-        gu = dot_nt(m16, dense_gu[...])
+    lane_f = lane.astype(F32)
+    mix = jnp.concatenate([dense_mix[...], jnp.zeros((1, 64), F32)], axis=1)
+    mix_hi = mix.astype(BF16).astype(F32)
+    row16 = iota((16, 128), 0)
+    mix_rows16 = jnp.where(row16 == 0, mix_hi, jnp.where(row16 == 1, mix - mix_hi, 0.0)).astype(BF16)
+
+    for r in range(4):
+        at = slice(r * block, (r + 1) * block)
+        lhs = quad_lhs(hops // 2 - 1, r)
+        squares = jnp.zeros((block, 128), F32)
+        for c in range(width // wide):
+            cols = slice(c * wide, (c + 1) * wide)
+            res = total[at, cols] + dot(lhs, quad_rhs(hops // 2 - 1, cols))
+            total[at, cols] = res
+            mixed[at, cols] = (res * gain_mid[:, cols]).astype(BF16)
+            sq = res * res
+            for i in range(wide // 128):
+                squares = squares + sq[:, 128 * i : 128 * i + 128]
+
+        scale = lax.rsqrt(jnp.sum(squares, axis=-1, keepdims=True) * (1.0 / width) + EPS)
+        scale_all[at, :] = jnp.broadcast_to(scale, (block, 128))
+        gu = dot_nt(mixed[at, :], dense_gu[...]) * scale
         hid = jnp.where(lane < 64, jax.nn.silu(gu) * pltpu.roll(gu, 64, 1), 0.0).astype(BF16)
-        hidden[pl.ds(base, block), :] = hid
-        row = jnp.sum(dot_nt(mix_rows, hid), axis=0, keepdims=True)
-        logit_all[me, :, pl.ds(base, block)] = row
-        return carry
-
-    lax.fori_loop(0, 4, mix_block, 0)
+        spread_lhs[at, :] = hid.astype(F32)
+        logit_pair[core, :, at] = jnp.sum(dot_nt(mix_rows16, hid), axis=0, keepdims=True)
+
+    def pair_copy(which):
+        ref = logit_pair.at[which]
+        return pltpu.make_async_remote_copy(
+            src_ref=ref,
+            dst_ref=ref,
+            send_sem=lp_send.at[0],
+            recv_sem=lp_recv.at[0],
+            device_id={"ep": partner},
+            device_id_type=MESH,
+        )
+
+    pair_copy(core).start()
 
     def logit_copy(j):
-        to = (me + j) % n
         return pltpu.make_async_remote_copy(
             src_ref=logit_all.at[me],
             dst_ref=logit_all.at[me],
-            send_sem=l_send.at[j],
-            recv_sem=l_recv.at[j],
-            device_id={"ep": to},
+            send_sem=l_send.at[0],
+            recv_sem=l_recv.at[0],
+            device_id={"ep": (me + j) % n},
             device_id_type=MESH,
         )
 
-    def logit_arrival(j):
-        source = (me - j + n) % n
+    def logit_rest():
+        ref = logit_all.at[pl.ds(0, n - 1)]
         return pltpu.make_async_remote_copy(
-            src_ref=logit_all.at[source],
-            dst_ref=logit_all.at[source],
-            send_sem=l_send.at[j],
-            recv_sem=l_recv.at[j],
-            device_id={"ep": source},
+            src_ref=ref,
+            dst_ref=ref,
+            send_sem=l_send.at[0],
+            recv_sem=l_recv.at[0],
+            device_id={"ep": partner},
             device_id_type=MESH,
         )
 
@@ -523,26 +573,34 @@
         logit_copy(j).start()
         return carry
 
-    lax.fori_loop(1, n, send_logit, 0)
-
-    def chosen(r):
-        extra = rows_all[pl.ds(r * per_block, per_block), :, width : width + 128]
+    def pick(r):
+        at = slice(r * block, (r + 1) * block)
+        extra = rows_all[r * per_block : (r + 1) * per_block, :, width : width + 128]
         extra = extra.astype(F32).reshape(block, 128)
         weight = jnp.sum(
             jnp.where((lane == me) | (lane == n + me), extra, 0.0), axis=-1, keepdims=True
         )
         spot = jnp.sum(jnp.where(lane == 2 * n + me, extra, 0.0), axis=-1, keepdims=True)
         source = (iota((block, 1), 0) // rows).astype(F32)
-        slot = jnp.where(spot > 0.5, source * cap + spot - 1.0, -1.0)
-        return weight, slot
-
-    lane_f = lane.astype(F32)
-    for r in range(4):
-        _, slot = chosen(r)
-        hot = jnp.where(lane_f == slot, 1.0, 0.0).T.astype(BF16)
+        slot = jnp.where(spot > 0.5, source * cap + spot - 1.0, -128.0)
+        hot = jnp.where(lane_f == slot, scale_all[at, :], 0.0).T[0:slots, :]
         picked[r * slots : (r + 1) * slots, :] = dot(
-            hot[0:slots, :], mixed[r * block : (r + 1) * block, :]
+            jnp.where(hot > 0.0, 1.0, 0.0).astype(BF16), mixed[at, :]
         ).astype(BF16)
+        scale_all[r * slots : (r + 1) * slots, :] = jnp.broadcast_to(
+            jnp.sum(hot, axis=-1, keepdims=True), (slots, 128)
+        )
+        spread_lhs[at, :] = jnp.where(lane_f == slot + 64.0, weight, spread_lhs[at, :])
+
+    pick(0)
+    pick(1)
+    pair_copy(other).wait_recv()
+    mine = pl.ds(pl.multiple_of(core * (seqs // 2), seqs // 2), seqs // 2)
+    logit_all[me] = logit_pair[0, :, mine] + logit_pair[1, :, mine]
+    lax.fori_loop(1, n, send_logit, 0)
+    pair_copy(core).wait_send()
+    pick(2)
+    pick(3)
     local[4].wait()
     local[5].wait()
     local[6].wait()
@@ -550,8 +608,9 @@
 
     def up_part(j, carry):
         cols = pl.ds(pl.multiple_of(j * fcut, fcut), fcut)
-        gated = jnp.minimum(dot(picked[...], w_gate[:, cols]), LIMIT)
-        up = jnp.clip(dot(picked[...], w_up[:, cols]), -LIMIT, LIMIT)
+        scale = scale_all[0 : 4 * slots, 0:1]
+        gated = jnp.minimum(dot(picked[...], w_gate[:, cols]) * scale, LIMIT)
+        up = jnp.clip(dot(picked[...], w_up[:, cols]) * scale, -LIMIT, LIMIT)
         active[:, cols] = ((up + 1.0) * gated * jax.nn.sigmoid(ALPHA * gated)).astype(BF16)
         return carry
 
@@ -568,59 +627,57 @@
 
     lax.fori_loop(0, width // wide, down_part, 0)
 
-    def take_logit(j, carry):
-        logit_arrival(j).wait_recv()
-        logit_copy(j).wait_send()
-        return carry
-
-    lax.fori_loop(1, n, take_logit, 0)
-    gate_row = jax.nn.sigmoid(jnp.sum(logit_all[...], axis=0))
+    logit_rest().wait_recv()
+    logit_rest().wait_send()
+    gates = logit_all[...].reshape(chips, 2, 1, seqs // 2)
+    gate_rows = [jax.nn.sigmoid(jnp.sum(gates[:, c], axis=0)) for c in range(2)]
+    for r in range(4):
+        row = gate_rows[r // 2][:, (r % 2) * block : (r % 2 + 1) * block]
+        gate = jnp.broadcast_to(row, (128, block)).T
+        at = slice(r * block, (r + 1) * block)
+        scaled = jnp.where(lane < 64, gate * spread_lhs[at, :], spread_lhs[at, :])
+        final_lhs[r] = scaled.astype(BF16)
+
+    quarter = chips // 4
 
     def hand_over(r):
-        ref = combined.at[other, pl.ds(r * (chips // 4), chips // 4)]
+        ref = combined.at[other, pl.ds(r * quarter, quarter)]
         return pltpu.make_async_remote_copy(
             src_ref=ref,
-            dst_ref=partner_part.at[pl.ds(r * (chips // 4), chips // 4)],
+            dst_ref=partner_part.at[pl.ds(r * quarter, quarter)],
             send_sem=cd_send.at[r],
             recv_sem=cd_recv.at[r],
             device_id={"ep": partner},
             device_id_type=MESH,
         )
 
-    for r in range(4):
-        at = slice(r * block, (r + 1) * block)
-        gate = jnp.broadcast_to(gate_row[:, at], (128, block)).T
-        weight, slot = chosen(r)
-        lhs = jnp.where(
-            lane < 64,
-            gate * hidden[at, :].astype(F32),
-            jnp.where(lane_f == slot + 64.0, jnp.where(slot >= 0.0, weight, 0.0), 0.0),
-        )
-        lhs = lhs[:, 0 : 64 + slots].astype(BF16)
-
-        def spread_part(j, carry, r=r, lhs=lhs):
-            cols = pl.ds(pl.multiple_of(j * wide, wide), wide)
+    far_block = ((chip + hops) % chips) // quarter
+
+    def combine(turn):
+        r = (far_block + turn) % 4
+        lhs = final_lhs[r, :, 0 : 64 + slots]
+
+        for j in range(width // wide):
+            cols = slice(j * wide, (j + 1) * wide)
             out = dot(lhs, down_rhs[r, :, cols]).astype(BF16)
-            out = out.reshape(per_block // 2, 2, rows, wide)
+            out = out.reshape(quarter, 2, rows, wide)
             for c in range(2):
-                combined[c, pl.ds(r * (chips // 4), chips // 4), :, cols] = out[:, c]
-            return carry
-
-        lax.fori_loop(0, width // wide, spread_part, 0)
+                combined[c, pl.ds(r * quarter, quarter), :, cols] = out[:, c]
         hand_over(r).start()
 
-    for r in range(4):
-        hand_over(r).wait_recv()
-
-    pieces = [(a, b) for a in range(2) for b in range(2)]
+    def handed(turn):
+        hand_over((far_block + turn) % 4).wait_recv()
+
+    pieces = [(a, b) for a in range(2) for b in range(4)]
+    part_w = width // 4
 
     def rs_copy(step, way, q):
         a, b = pieces[q]
         return pltpu.make_async_remote_copy(
-            src_ref=ring_out.at[way, step, pl.ds(a * half_rows, half_rows), pl.ds(b * half_w, half_w)],
-            dst_ref=ring_in.at[way, step, pl.ds(a * half_rows, half_rows), pl.ds(b * half_w, half_w)],
+            src_ref=ring_out.at[way, step, pl.ds(a * half_rows, half_rows), pl.ds(b * part_w, part_w)],
+            dst_ref=ring_in.at[way, step, pl.ds(a * half_rows, half_rows), pl.ds(b * part_w, part_w)],
             send_sem=r_send.at[way, q],
-            recv_sem=r_recv.at[way, step, q],
+            recv_sem=(recv_a if q < 4 else recv_b).at[way, step, q % 4],
             device_id={"ep": nexts[way]},
             device_id_type=MESH,
         )
@@ -628,12 +685,12 @@
     def rs_own(dist, way, q):
         a, b = pieces[q]
         to = (chip + dist) % chips if way == 0 else (chip - dist + chips) % chips
-        rr, cc = pl.ds(a * half_rows, half_rows), pl.ds(b * half_w, half_w)
+        rr, cc = pl.ds(a * half_rows, half_rows), pl.ds(b * part_w, part_w)
         return combined[core, to, rr, cc].astype(F32) + partner_part[to, rr, cc].astype(F32)
 
     def rs_step(step, way, q, got, used):
         a, b = pieces[q]
-        rr, cc = pl.ds(a * half_rows, half_rows), pl.ds(b * half_w, half_w)
+        rr, cc = pl.ds(a * half_rows, half_rows), pl.ds(b * part_w, part_w)
         value = rs_own(hops - step, way, q)
         if got:
             rs_copy(step - 1, way, q).wait_recv()
@@ -643,39 +700,73 @@
         ring_out[way, step, rr, cc] = value.astype(BF16)
         rs_copy(step, way, q).start()
 
-    halves = (range(0, 2), range(2, 4))
-    for i in range(2):
+    halves = (range(0, 4), range(4, 8))
+    combine(0)
+    combine(1)
+    handed(0)
+    for i in range(4):
         for way in (0, 1):
             rs_step(0, way, halves[way][i], False, False)
-    for i in range(2):
+    combine(3)
+    handed(1)
+    handed(3)
+    for i in range(4):
         for way in (0, 1):
             rs_step(1, way, halves[1 - way][i], False, False)
-    for i in range(2):
+    combine(2)
+    for i in range(4):
         for way in (0, 1):
             rs_step(1, way, halves[way][i], True, True)
+    handed(2)
 
     def rs_body(step, carry):
-        for q in range(4):
+        for q in range(8):
             for way in (0, 1):
                 rs_step(step, way, q, True, True)
         return carry
 
     lax.fori_loop(2, hops, rs_body, 0)
-    for q in range(4):
+    own_rows = pl.ds(pl.multiple_of(me * rows, rows), rows)
+    for q in range(8):
         a, b = pieces[q]
-        rr, cc = pl.ds(a * half_rows, half_rows), pl.ds(b * half_w, half_w)
-        value = rs_own(0, 0, q) + own_res[rr, cc]
+        rr, cc = pl.ds(a * half_rows, half_rows), pl.ds(b * part_w, part_w)
+        value = rs_own(0, 0, q) + total[own_rows, :][a * half_rows : (a + 1) * half_rows, b * part_w : (b + 1) * part_w]
         for way in (0, 1):
             rs_copy(hops - 1, way, q).wait_recv()
             value = value + ring_in[way, hops - 1, rr, cc].astype(F32)
         layer_out[rr, cc] = value.astype(BF16)
-    for q in range(4):
+    for q in range(8):
         for way in (0, 1):
             rs_copy(hops - 1, way, q).wait_send()
     for r in range(4):
         hand_over(r).wait_send()
     for c in outs:
         c.wait()
+
+
+def write_out(sources, targets, buffers, in_sem, out_sem):
+    count = len(sources)
+    takes = [pltpu.make_async_copy(sources[i], buffers[i], in_sem.at[i]) for i in range(count)]
+    gives = [pltpu.make_async_copy(buffers[i], targets[i], out_sem.at[i]) for i in range(count)]
+    for take in takes:
+        take.start()
+    for take, give in zip(takes, gives):
+        take.wait()
+        give.start()
+    for give in gives:
+        give.wait()
+
+
+def finish(a, b, c, out_a, out_b, out_c, va, vb, vc, in_sem, out_sem):
+    half = b.shape[0] // 2
+    cuts = [pl.ds(0, half), pl.ds(half, half)]
+    write_out(
+        [b.at[cut] for cut in cuts] + [c.at[cut] for cut in cuts] + [a],
+        [out_b.at[cut] for cut in cuts] + [out_c.at[cut] for cut in cuts] + [out_a],
+        [vb.at[cut] for cut in cuts] + [vc.at[cut] for cut in cuts] + [va],
+        in_sem,
+        out_sem,
+    )
 
 
 def on_device(
@@ -712,15 +803,6 @@
     cap = max(2, 2 * rows * top // n)
     chips, hops, block = n // 2, n // 4, seqs // 4
     slots = (n // 4) * cap
-    params = jnp.stack(
-        [
-            decay_rate.reshape(128),
-            frequency.reshape(128),
-            jnp.repeat(log_step, 64),
-            jnp.tile(skip_gain.reshape(32), 4),
-            jnp.pad(dense_mix, (0, 64)),
-        ]
-    )
     operands = (
         tokens,
         routes.T,
@@ -729,7 +811,11 @@
         state_imag.transpose(1, 2, 0).reshape(128, seqs),
         gain_in[None],
         proj_in.T,
-        params,
+        decay_rate,
+        frequency,
+        log_step[None],
+        skip_gain,
+        dense_mix[None],
         input_real.transpose(0, 2, 1).reshape(32, 64),
         input_imag.transpose(0, 2, 1).reshape(32, 64),
         output_real.reshape(32, 64),
@@ -745,37 +831,14 @@
     )
     vmem = pl.BlockSpec(memory_space=pltpu.VMEM)
     far = pl.BlockSpec(memory_space=pl.ANY)
-    in_specs = [
-        far,
-        vmem,
-        vmem,
-        far,
-        far,
-        vmem,
-        far,
-        vmem,
-        vmem,
-        vmem,
-        vmem,
-        vmem,
-        far,
-        vmem,
-        far,
-        far,
-        far,
-        far,
-        far,
-        far,
-    ]
+    in_specs = [far] + [vmem] * 2 + [far] * 2 + [vmem, far] + [vmem] * 9 + [far, vmem] + [far] * 6
     V = pltpu.VMEM
     dma = pltpu.SemaphoreType.DMA
     scratch = [
         V((n, rows, width + 128), BF16),
         V((n, 32, width), BF16),
         V((n, block, 128), BF16),
-        V((seqs, n * 32), BF16),
-        V((block, width), F32),
-        V((rows, width), F32),
+        V((seqs, width), F32),
         V((seqs, width), BF16),
         V((width, ff), BF16),
         V((width, ff), BF16),
@@ -785,6 +848,7 @@
         V((128, seqs), F32),
         V((128, seqs), F32),
         V((4 * slots, width), BF16),
+        V((4, block, 128), BF16),
         V((4 * slots, ff), BF16),
         V((4, 64 + slots, width), BF16),
         V((2, chips, rows, width), BF16),
@@ -794,25 +858,17 @@
         V((seqs, 128), F32),
         V((128, width), BF16),
         V((128, width), BF16),
-        V((seqs, 128), BF16),
-        V((n, 1, seqs), F32),
+        V((seqs, 128), F32),
+        V((seqs, 128), F32),
+        V((2, 1, seqs), F32),
+        V((n, 1, seqs // 2), F32),
         V((128, 128), F32),
         dma((17,)),
         dma((2,)),
-        dma((2, 4)),
-        dma((2, hops, 4)),
-        dma((2, 2)),
-        dma((2, hops, 2)),
-        dma((2, 2)),
-        dma((2, hops, 2)),
-        dma((2, 2)),
-        dma((2, hops, 2)),
-        dma((2, 4)),
-        dma((2, hops, 4)),
     ]
-    for _ in range(4):
-        scratch += [dma((2,)), dma((2, hops + 1))]
-    scratch += [dma((4,)), dma((4,)), dma((n,)), dma((n,))]
+    scratch += [dma((2, count)) for count in (4, 2, 4, 4, 8)]
+    scratch += [dma((2, hops, 4))] * 2 + [dma((2,))] * 4 + [dma((2, hops + 1))] * 2
+    scratch += [dma((4,)), dma((4,))] + [dma((1,))] * 4
     layer_out, new_re, new_im = pl.pallas_call(
         functools.partial(kernel, n, (rows, width, ff, cap)),
         out_shape=(
@@ -828,6 +884,18 @@
         ),
         name="layer_step",
     )(*operands)
+    layer_out, new_re, new_im = pl.pallas_call(
+        finish,
+        out_shape=(
+            jax.ShapeDtypeStruct((rows, width), BF16),
+            jax.ShapeDtypeStruct((128, seqs), F32),
+            jax.ShapeDtypeStruct((128, seqs), F32),
+        ),
+        in_specs=(far,) * 3,
+        out_specs=(far,) * 3,
+        scratch_shapes=[V((rows, width), BF16), V((128, seqs), F32), V((128, seqs), F32), dma((5,)), dma((5,))],
+        name="write_out",
+    )(layer_out, new_re, new_im)
     groups, state = state_real.shape[1:]
 
     def back(values):

time: 155 us -> 133 us (0.86)
  Pallas kernels: 144 us -> 132 us
  local copies, waits for them, and re-layouts: 9.77 us -> 0 us
    pallas_call x1, Pallas kernels: 144 us -> 130 us  [on_device(): pl.pallas_call(functools.partial(kernel, n, (rows, width, ff, cap)), out_...]
    unnamed x3 -> x0, local copies, waits for them, and re-layouts: 5.34 us -> none
    another operation x8 -> x0, local copies, waits for them, and re-layouts: 3.72 us -> none  [the longest x6 2.96 us: on_device(): jnp.stack([decay_rate.reshape(128), frequency.reshape(128), jnp.repeat(lo...]
    pallas_call x0 -> x1, Pallas kernels: none -> 2.04 us  [on_device(): pl.pallas_call(finish, out_shape=(jax.ShapeDtypeStruct((rows, width), BF1...]
where the time goes in v2:
time: 133 us
  Pallas kernels  132 us (99%)
    pallas_call x1, Pallas kernels, on_device(): pl.pallas_call(functools.partial(kernel, n, (rows, width, ff, cap)), out_...  130 us

profile of v2, /device:TPU:86, one launch (start us, length us, event | category | flops | bytes accessed | tf_op | source)
XLA Modules:
  0.0 133.0 jit_solution(1063221325681672471)
XLA Ops:
  0.6 130.2 %layer_step.1 = (bf16[32,2048]{1,0:T(8,128)(2,1)}, f32[128,1024]{1,0:T(8,128)}, f32[128,1024]{1,0:T(8,128)}) custom-call(bf16[32,2048]{1,0:T(8,128)(2,1)} %tokens.1, s32[4,32]{1,0:T(4,128)} %bitcast.46, f32[4,32]{1,0:T(4,128)} %bitcast.47, f32[128,1024]{1,0:T(8,128)} %bitcast.35, f32[128,1024]{1,0:T(8,128)} %bitcast.36, f32[1,2048]{1,0:T(1,128)} %bitcast.44, ...), custom_call_target="tpu_custom_call" | custom-call | tf_op jit(solution)/shard_map/layer_step/pallas_call | solution.py:872
  130.8 2.0 %write_out.1 = (bf16[32,2048]{1,0:T(8,128)(2,1)}, f32[128,1024]{1,0:T(8,128)}, f32[128,1024]{1,0:T(8,128)}) custom-call(bf16[32,2048]{1,0:T(8,128)(2,1)} %get-tuple-element.9.a, f32[128,1024]{1,0:T(8,128)} %get-tuple-element.10.b, f32[128,1024]{1,0:T(8,128)} %get-tuple-element.11.c), custom_call_target="tpu_custom_call" | custom-call | tf_op jit(solution)/shard_map/write_out/pallas_call | solution.py:887
